TPU v7x, 256 devices: a whole 4x4x8 slice. The times are simulated.
256 devices in a mesh: sp: 16 (over y, x), tp: 16 (over z, core).
Axes of the slice: x: 4, y: 4, z: 8, core: 2. Of those that a mesh axis runs over, the one named last changes fastest.
Arguments:
- saved_input: bfloat16 [4096, 2048], P('sp'), may hold values from -6 to 6
- cotangent: bfloat16 [4096, 2048], P('sp'), may hold values from -6 to 6
- expert_ids: int32 [4096, 2], P('sp'), may hold values from 0 to 15, all different within a row; in each aligned block of 256 rows (0 to 255, 256 to 511, ...) at most 64 rows name the same one
- route_weight: float32 [4096, 2], P('sp'), may hold values from 0.1 to 0.9
- w_gate: bfloat16 [16, 2048, 6144], P('sp', None, 'tp'), may hold values from -0.125 to 0.125
- w_up: bfloat16 [16, 2048, 6144], P('sp', None, 'tp'), may hold values from -0.125 to 0.125
- w_down: bfloat16 [16, 6144, 2048], P('sp', 'tp'), may hold values from -0.078125 to 0.078125
- w_out: bfloat16 [2048, 2048], P(None, 'tp'), may hold values from -0.125 to 0.125
- channel_gain: float32 [2048], P('tp'), may hold values from 0.1 to 1.9
- conv_taps: float32 [31, 2048], P(None, 'tp'), may hold values from -1 to 1
- glu_value: bfloat16 [2048, 4096], P('tp', 'sp'), may hold values from -6 to 6
- glu_gate: bfloat16 [2048, 4096], P('tp', 'sp'), may hold values from -8 to 8
- conv_out: bfloat16 [2048, 4096], P('tp', 'sp'), may hold values from -6 to 6
- norm_mean: float32 [4096], P('sp'), may hold values from -3 to 3
- norm_rstd: float32 [4096], P('sp'), may hold values from 0.5 to 2
Outputs:
- gate_grad: bfloat16 [16, 2048, 6144], P('sp', None, 'tp')
- up_grad: bfloat16 [16, 2048, 6144], P('sp', None, 'tp')
- down_grad: bfloat16 [16, 6144, 2048], P('sp', 'tp')
- proj_grad: float32 [2048, 2048], P('sp', 'tp')
- value_grad: bfloat16 [2048, 4096], P('tp', 'sp')
- gate_in_grad: bfloat16 [2048, 4096], P('tp', 'sp')
Inputs may be any that keep to these rules, and one draw needn't show every extreme that they name: `expert_ids`: the two experts of a position differ. In the positions of one block of 256, no expert is named more than 64 times, a bound that some block reaches.
All inputs are finite; a program needn't handle non-finite values.
Results may differ from a plain program's by a relative error of at most 0.018.
Values may be sent and summed in bfloat16 or wider, within the bound.
No kernel may reach another device: no remote copies, remote signals or barrier semaphores. Data moves between devices by JAX's collectives and lax.ppermute only.
A program may use at most 128 MiB of HBM per device.

v0:
```python
import jax
import jax.numpy as jnp
from jax import lax
from jax.sharding import PartitionSpec as P

D = 2048
C = 2048


def in_one_piece(arrays, axis, split_dim, concat_dim, along):
    ends, at = ([], 0)
    for a in arrays[:-1]:
        at += a.shape[along]
        ends.append(at)
    both = jnp.concatenate(arrays, axis=along)
    return tuple(
        jnp.split(
            lax.all_to_all(both, axis, split_axis=split_dim, concat_axis=concat_dim, tiled=True),
            ends,
            axis=along,
        )
    )


def cut_along(value, dim, devices):
    before, after = (value.shape[:dim], value.shape[dim + 1 :])
    return jnp.moveaxis(value.reshape(*before, devices, -1, *after), dim, 0)


def sent_and_summed(value, axis, dim):
    devices = lax.axis_size(axis)
    tiles = lax.all_to_all(cut_along(value, dim, devices), axis, 0, 0, tiled=True)
    return jnp.sum(tiles.astype(jnp.float32), axis=0)


def copy_for_each(value, axis):
    copies = jnp.broadcast_to(value, (lax.axis_size(axis), *value.shape))
    return lax.all_to_all(copies, axis, split_axis=0, concat_axis=0, tiled=True)


def of_everyone(value, axis):
    everything = copy_for_each(value, axis)
    return jnp.sum(everything, axis=0)


def in_one(arrays, axis):
    ravelled, at, gathered = (jnp.concatenate([a.reshape(-1) for a in arrays]), 0, [])
    subtotal = of_everyone(ravelled, axis)
    for a in arrays:
        gathered.append(subtotal[at : at + a.size].reshape(a.shape))
        at += a.size
    return tuple(gathered)


def from_behind(value, axis, by):
    devices = lax.axis_size(axis)
    pairs = [(i, i + by) for i in range(devices) if 0 <= i + by < devices]
    return lax.ppermute(value, axis, pairs)


def contract(left, right, left_dim, right_dim):
    return lax.dot_general(
        left, right, (((left_dim,), (right_dim,)), ((), ())), preferred_element_type=jnp.float32
    )


def expert_grads(rows_in, rows_cot, gate_weight, up_weight, down_weight):
    gate_pre = jnp.dot(rows_in, gate_weight, preferred_element_type=jnp.float32)
    up_pre = jnp.dot(rows_in, up_weight, preferred_element_type=jnp.float32)
    sigma = jax.nn.sigmoid(gate_pre)
    hidden = (gate_pre * sigma * up_pre).astype(jnp.bfloat16)
    hidden_cot = contract(rows_cot, down_weight, 1, 1)
    down_part = contract(hidden, rows_cot, 0, 0).astype(jnp.bfloat16)
    gate_cot = (hidden_cot * up_pre * sigma * (1.0 + gate_pre * (1.0 - sigma))).astype(jnp.bfloat16)
    up_cot = (hidden_cot * gate_pre * sigma).astype(jnp.bfloat16)
    gate_part = contract(rows_in, gate_cot, 0, 0).astype(jnp.bfloat16)
    up_part = contract(rows_in, up_cot, 0, 0).astype(jnp.bfloat16)
    input_cot = contract(gate_cot, gate_weight, 1, 1) + contract(up_cot, up_weight, 1, 1)
    return (gate_part, up_part, down_part, input_cot)


def on_device(
    saved_input,
    cotangent,
    expert_ids,
    route_weight,
    w_gate,
    w_up,
    w_down,
    w_out,
    channel_gain,
    conv_taps,
    glu_value,
    glu_gate,
    conv_out,
    norm_mean,
    norm_rstd,
):
    tokens_here = cotangent.shape[0]
    sp_count = lax.axis_size("sp")
    local_experts = w_gate.shape[0]
    expert_count = local_experts * sp_count
    capacity = 4 * tokens_here // expert_count
    pairs = expert_ids.reshape(2 * tokens_here)
    onehot = (pairs[:, None] == jnp.arange(expert_count, dtype=jnp.int32)[None, :]).astype(
        jnp.int32
    )
    before = jnp.cumsum(onehot, axis=0) - onehot
    target = pairs * capacity + jnp.sum(before * onehot, axis=1)
    owner = (
        jnp.zeros((expert_count * capacity,), jnp.int32)
        .at[target]
        .set(jnp.arange(2 * tokens_here, dtype=jnp.int32) + 1)
    )
    filled = (owner > 0)[:, None]
    pair_index = jnp.maximum(owner - 1, 0)
    scaled = (route_weight[:, :, None] * cotangent.astype(jnp.float32)[:, None, :]).astype(
        jnp.bfloat16
    )
    scaled = scaled.reshape(2 * tokens_here, D)
    send_cot = jnp.where(filled, scaled[pair_index], jnp.zeros_like(scaled[:1])).reshape(
        expert_count, capacity, D
    )
    send_in = jnp.where(filled, saved_input[pair_index // 2], jnp.zeros_like(saved_input[:1]))
    send_in = send_in.reshape(expert_count, capacity, D)
    rows_cot, rows_in = in_one_piece((send_cot, send_in), "sp", 0, 1, 2)
    results = [expert_grads(rows_in[0], rows_cot[0], w_gate[0], w_up[0], w_down[0])]
    gate_grad = jnp.stack([result[0] for result in results])
    up_grad = jnp.stack([result[1] for result in results])
    down_grad = jnp.stack([result[2] for result in results])
    input_cot = jnp.stack([result[3] for result in results])
    blocks = input_cot.reshape(local_experts, sp_count, capacity, D)
    share = lax.psum_scatter(
        blocks.astype(jnp.bfloat16), "tp", scatter_dimension=2, tiled=True
    ).astype(jnp.float32)
    returned = lax.all_to_all(
        share.astype(jnp.bfloat16), "sp", split_axis=1, concat_axis=0, tiled=True
    ).astype(share.dtype)
    whole = lax.all_gather(returned.astype(jnp.bfloat16), "tp", axis=2, tiled=True).astype(
        returned.dtype
    )
    routed = whole.reshape(expert_count * capacity, D)[target].reshape(tokens_here, 2, D)
    summed = jnp.sum(routed, axis=1)
    mixed_cot = (cotangent.astype(jnp.float32) + summed).astype(jnp.bfloat16)
    centered = (conv_out.astype(jnp.float32) - norm_mean[None, :]) * norm_rstd[None, :]
    normed = centered * channel_gain[:, None]
    sigma = jax.nn.sigmoid(normed)
    output_act = (normed * sigma).astype(jnp.bfloat16)
    proj_grad = sent_and_summed(contract(mixed_cot, output_act, 0, 1).astype(jnp.bfloat16), "sp", 0)
    act_cot = contract(w_out, mixed_cot, 0, 1)
    norm_cot = act_cot * sigma * (1.0 + normed * (1.0 - sigma)) * channel_gain[:, None]
    first_sum, second_sum = in_one(
        (jnp.sum(norm_cot, axis=0), jnp.sum(norm_cot * centered, axis=0)), "tp"
    )
    conv_cot = norm_rstd[None, :] * (
        norm_cot - first_sum[None, :] / C - centered * second_sum[None, :] / C
    )
    reach = conv_taps.shape[0] - 1
    rim = from_behind(conv_cot[:, :reach], "sp", -1)
    padded = jnp.concatenate([conv_cot, rim], axis=1)
    glu_cot = conv_taps[0][:, None] * padded[:, :tokens_here]
    for lag in range(1, reach + 1):
        glu_cot = glu_cot + conv_taps[lag][:, None] * padded[:, lag : lag + tokens_here]
    gate_sigma = jax.nn.sigmoid(glu_gate.astype(jnp.float32))
    value_grad = (glu_cot * gate_sigma).astype(jnp.bfloat16)
    gate_in_grad = (
        glu_cot * glu_value.astype(jnp.float32) * gate_sigma * (1.0 - gate_sigma)
    ).astype(jnp.bfloat16)
    return (gate_grad, up_grad, down_grad, proj_grad, value_grad, gate_in_grad)


def solution(mesh):
    in_specs = (
        P("sp", None),
        P("sp", None),
        P("sp", None),
        P("sp", None),
        P("sp", None, "tp"),
        P("sp", None, "tp"),
        P("sp", "tp", None),
        P(None, "tp"),
        P("tp"),
        P(None, "tp"),
        P("tp", "sp"),
        P("tp", "sp"),
        P("tp", "sp"),
        P("sp"),
        P("sp"),
    )
    out_specs = (
        P("sp", None, "tp"),
        P("sp", None, "tp"),
        P("sp", "tp", None),
        P("sp", "tp"),
        P("tp", "sp"),
        P("tp", "sp"),
    )
    return jax.shard_map(
        on_device, mesh=mesh, in_specs=in_specs, out_specs=out_specs, check_vma=False
    )
```

profile of v0, /device:TPU:24, one launch (start us, length us, event | category | flops | bytes accessed | tf_op | source)
XLA Modules:
  0.0 370.5 jit_solution(13635867785435302561)
XLA Ops:
  7.2 0.0 copy-start
  7.2 0.0 reduce-scatter.2.cloned.1.call-start
  7.2 0.8 broadcast_multiply_fusion
  8.0 0.8 copy.65
  8.8 0.1 eq.25
  9.0 0.1 eq.29
  9.1 0.1 copy.64
  9.3 0.1 mul.436
  9.4 1.2 reduce-window.6
  10.6 0.2 slice_reduce_fusion
  10.9 0.1 fusion.114
  11.0 2.4 scatter_custom_fusion
  13.5 5.3 %mul.440 = f32[256,2,2048]{2,1,0:T(2,128)} broadcast(bf16[256,2048]{1,0:T(8,128)(2,1)} %param.16), dimensions={0,2} | broadcast | bytes 5242880 | tf_op jit(solution)/shard_map/mul | solution.py:117
  18.8 6.1 %mul.441 = f32[512,2048]{1,0:T(8,128)} reshape(f32[256,2,2048]{2,1,0:T(2,128)} %mul.440) | data formatting | bytes 8388608 | tf_op jit(solution)/shard_map/mul | solution.py:117
  24.9 0.1 copy.68
  25.0 0.1 mul.438
  25.2 0.1 broadcast_in_dim.46
  25.2 3.8 %multiply_convert_fusion = bf16[512,2048]{1,0:T(8,128)(2,1)} fusion(f32[512,2048]{1,0:T(8,128)} %mul.441, f32[512]{0:T(512)S(1)} %mul.438), kind=kLoop, calls=%fused_computation.8 | loop fusion | flops 2097152 | bytes 6293504 | tf_op jit(solution)/shard_map/convert_element_type | solution.py:117
  29.0 10.8 %gather_fusion = bf16[1024,2048]{1,0:T(8,128)(2,1)} fusion(bf16[512,2048]{1,0:T(8,128)(2,1)} %multiply_convert_fusion, s32[1024]{0:T(1024)S(1)} %get-tuple-element.73), kind=kCustom, calls=%fused_computation | custom fusion | bytes 8392704 | tf_op jit(solution)/shard_map/gather | solution.py:121
  39.8 6.0 %gather_fusion.1 = bf16[1024,2048]{1,0:T(8,128)(2,1)} fusion(bf16[256,2048]{1,0:T(8,128)(2,1)S(1)} %copy-done.2, s32[1024]{0:T(1024)S(1)} %get-tuple-element.74), kind=kCustom, calls=%fused_computation.1 | custom fusion | bytes 8392704 | tf_op jit(solution)/shard_map/gather | solution.py:124
  45.8 5.8 %broadcast_select_fusion.1 = (bf16[16,64,2048]{2,1,0:T(8,128)(2,1)}, bf16[16,64,2048]{2,1,0:T(8,128)(2,1)}) fusion(bf16[16,64,2048]{2,1,0:T(8,128)(2,1)} %bitcast.144, pred[16,64]{1,0:T(8,128)(4,1)S(1)} %broadcast_in_dim.46, bf16[16,64,2048]{2,1,0:T(8,128)(2,1)} %bitcast.145), kind=kLoop, calls=%fused_computation.10 | loop fusion | flops 4194304 | bytes 16778240 | tf_op jit(solution)/shard_map/jit(_where)/select_n | solution.py:121
  51.6 7.8 %pad_maximum_fusion = bf16[16,64,4096]{2,1,0:T(8,128)(2,1)} fusion(bf16[16,64,2048]{2,1,0:T(8,128)(2,1)} %get-tuple-element.78, bf16[16,64,2048]{2,1,0:T(8,128)(2,1)} %get-tuple-element.77), kind=kLoop, calls=%fused_computation.4 | loop fusion | flops 16777216 | bytes 16777216 | tf_op jit(solution)/shard_map/concatenate | solution.py:15
  59.4 101.1 %all_to_all.35 = bf16[16,64,4096]{2,1,0:T(8,128)(2,1)S(1)} all-to-all(bf16[16,64,4096]{2,1,0:T(8,128)(2,1)} %pad_maximum_fusion), channel_id=1, replica_groups=mesh['sp'=16,'tp'=16] {'sp'}, dimensions={0} | all-to-all | bytes 16777216 | tf_op jit(solution)/shard_map/all_to_all | solution.py:18
  160.6 2.3 fusion.3
  162.9 0.2 copy-done.5
  163.1 2.3 fusion.4
  165.5 0.2 copy-done.15
  165.7 2.8 multiply_convert_fusion.2
  168.5 2.4 fusion.8
  170.9 2.4 add_convert_fusion
  173.3 4.3 %copy.69 = bf16[1,16,64,2048]{3,1,0,2:T(8,128)(2,1)} copy(bf16[1,16,64,2048]{3,2,1,0:T(8,128)(2,1)S(1)} %bitcast.146) | data formatting | bytes 8388608 | tf_op jit(solution)/shard_map/convert_element_type | solution.py:134
  177.6 0.0 reduce-scatter.2.cloned.1.call-update
  177.6 0.0 all-gather.3.cloned.1.call-start
  177.6 64.5 %reduce-scatter.2.cloned.1.call-done = bf16[1,16,4,2048]{3,1,0,2:T(8,128)(2,1)} async-done(((bf16[1,16,64,2048]{3,1,0,2:T(8,128)(2,1)}), bf16[1,16,4,2048]{3,1,0,2:T(8,128)(2,1)}) %reduce-scatter.2.cloned.1.call-update) | async-done | bytes 262160 | tf_op jit(solution)/shard_map/reduce_scatter | solution.py:133
  242.2 1.2 copy.70
  243.3 13.6 %all_to_all.36 = bf16[1,16,4,2048]{3,2,0,1:T(4,128)(2,1)S(1)} all-to-all(bf16[1,16,4,2048]{3,2,0,1:T(4,128)(2,1)S(1)} %copy.70), channel_id=1, replica_groups=mesh['sp'=16,'tp'=16] {'sp'}, dimensions={1} | all-to-all | bytes 524288 | tf_op jit(solution)/shard_map/all_to_all | solution.py:136
  256.9 0.9 copy.71
  257.8 0.0 all-gather.3.cloned.1.call-update
  257.8 0.1 copy.73
  257.9 0.1 copy.76
  258.1 0.1 copy.75
  258.3 0.0 copy-start.19
  258.3 5.9 %fusion.5 = bf16[1,2048,384]{2,1,0:T(8,128)(2,1)} fusion(bf16[1024,384]{1,0:T(8,128)(2,1)S(1)} %get-tuple-element.41, bf16[1,1024,4096]{2,1,0:T(8,128)(2,1)} %bitcast.150), kind=kOutput, calls=%fused_computation.18 | convolution fusion | flops 1611399168 | bytes 6553600 | tf_op jit(solution)/shard_map/dot_general | solution.py:62
  264.1 5.4 %fusion.7 = bf16[1,384,2048]{2,1,0:T(8,128)(2,1)} fusion(bf16[1,1024,4096]{2,1,0:T(8,128)(2,1)} %bitcast.151, f32[1024,384]{1,0:T(8,128)S(1)} %copy-done.19, f32[1024,384]{1,0:T(8,128)S(1)} %copy-done.17), kind=kOutput, calls=%fused_computation.20 | convolution fusion | flops 1613758464 | bytes 8912896 | tf_op jit(solution)/shard_map/dot_general | solution.py:62
  269.5 26.8 %all-gather.3.cloned.1.call-done = bf16[1,16,64,2048]{3,1,0,2:T(8,128)(2,1)} async-done(((bf16[1,16,4,2048]{3,1,0,2:T(8,128)(2,1)}), bf16[1,16,64,2048]{3,1,0,2:T(8,128)(2,1)}) %all-gather.3.cloned.1.call-update) | async-done | bytes 4194320 | tf_op jit(solution)/shard_map/all_gather | solution.py:139
  296.3 7.8 %copy.72 = f32[1,16,64,2048]{3,2,1,0:T(8,128)} copy(bf16[1,16,64,2048]{3,1,0,2:T(8,128)(2,1)} %all-gather.3.cloned.1.call-done) | data formatting | bytes 12582912 | tf_op jit(solution)/shard_map/reshape | solution.py:142
  304.2 8.8 %gather_fusion.2 = f32[512,2048]{1,0:T(8,128)} fusion(f32[1024,2048]{1,0:T(8,128)} %bitcast.143, s32[1024]{0:T(1024)S(1)} %pad_clamp_fusion), kind=kCustom, calls=%fused_computation.2 | custom fusion | bytes 8390656 | tf_op jit(solution)/shard_map/gather | solution.py:142
  312.9 6.0 %reshape.159 = f32[256,2,2048]{2,1,0:T(2,128)} reshape(f32[512,2048]{1,0:T(8,128)} %gather_fusion.2) | data formatting | bytes 8388608 | tf_op jit(solution)/shard_map/reshape | solution.py:142
  319.0 0.0 copy-start.3
  319.0 0.0 copy-start.6
  319.0 8.6 %reduce_sum.58 = f32[256,2048]{1,0:T(8,128)} reduce(f32[256,2,2048]{2,1,0:T(2,128)} %reshape.159, f32[]{:T(128)} %constant.44.clone.1), dimensions={1}, to_apply=%region_5.6 | reduce | flops 524288 | bytes 6291460 | tf_op jit(solution)/shard_map/reduce_sum | solution.py:143
  327.7 2.1 fusion.123
  329.8 0.6 broadcast_in_dim.51
  330.5 4.4 %all-to-all-start.3 = ((f32[16,1,512]{2,1,0:T(1,128)}), f32[16,1,512]{2,1,0:T(1,128)S(1)}, u32[]{:S(2)}, u32[]{:S(2)}) async-start(f32[16,1,512]{2,1,0:T(1,128)} %broadcast_in_dim.51), calls=%async_computation.4 | async-start | bytes 65536 | tf_op jit(solution)/shard_map/all_to_all | solution.py:38
  334.9 3.1 convolution_convert_fusion.2
  337.9 4.6 %all-to-all-done.3 = f32[16,1,512]{2,1,0:T(1,128)S(1)} async-done(((f32[16,1,512]{2,1,0:T(1,128)}), f32[16,1,512]{2,1,0:T(1,128)S(1)}, u32[]{:S(2)}, u32[]{:S(2)}) %all-to-all-start.3) | async-done | bytes 32800 | tf_op jit(solution)/shard_map/all_to_all | solution.py:38
  342.5 7.2 %all-to-all-start.2 = ((bf16[16,128,128]{2,1,0:T(8,128)(2,1)}), bf16[16,128,128]{2,1,0:T(8,128)(2,1)S(1)}, u32[]{:S(2)}, u32[]{:S(2)}) async-start(bf16[16,128,128]{2,1,0:T(8,128)(2,1)} %bitcast.16), calls=%async_computation.3 | async-start | bytes 1048576 | tf_op jit(solution)/shard_map/all_to_all | solution.py:32
  349.8 0.2 subtract_multiply_fusion
  350.0 4.9 %collective-permute-start = (f32[128,30]{0,1:T(8,128)S(1)}, f32[128,30]{0,1:T(8,128)S(1)}, u32[]{:S(2)}, u32[]{:S(2)}) collective-permute-start(f32[128,30]{0,1:T(8,128)S(1)} %slice.271), channel_id=1, source_target_pairs={{16,0},{32,16},{48,32},{64,48},{80,64},{96,80},{112,96},{128,112},... | collective-permute-start | bytes 46088 | tf_op jit(solution)/shard_map/ppermute | solution.py:58
  354.9 5.8 %fusion.6 = bf16[1,2048,384]{2,1,0:T(8,128)(2,1)} fusion(bf16[1024,384]{1,0:T(8,128)(2,1)S(1)} %get-tuple-element.40, bf16[1,1024,4096]{2,1,0:T(8,128)(2,1)} %bitcast.152), kind=kOutput, calls=%fused_computation.19 | convolution fusion | flops 1611399168 | bytes 6553600 | tf_op jit(solution)/shard_map/dot_general | solution.py:62
  360.8 0.4 multiply_convert_fusion.5
  361.2 0.7 copy.77
  362.0 0.7 copy.78
  362.7 0.7 convert_reduce_fusion
  (51 shorter events, 0.3 us)
Async XLA Ops:
  7.2 153.4 %copy-start = (bf16[1,2048,384]{2,1,0:T(8,128)(2,1)S(1)}, bf16[1,2048,384]{2,1,0:T(8,128)(2,1)}, u32[]{:S(2)}) copy-start(bf16[1,2048,384]{2,1,0:T(8,128)(2,1)} %param.19) | copy-start | bytes 4718596
  7.2 235.0 %reduce-scatter.2.cloned.1.call-start = ((), (), s32[]{:S(2)}) async-start(), calls=%async_computation.5 | async-start | bytes 4456448 | tf_op jit(solution)/shard_map/reduce_scatter | solution.py:133
  18.8 6.1 %copy-start.13 = (f32[256,2]{0,1:T(2,128)S(1)}, f32[256,2]{0,1:T(2,128)}, u32[]{:S(2)}) copy-start(f32[256,2]{0,1:T(2,128)} %param.18) | copy-start | bytes 6148
  29.0 10.8 %copy-start.2 = (bf16[256,2048]{1,0:T(8,128)(2,1)S(1)}, bf16[256,2048]{1,0:T(8,128)(2,1)}, u32[]{:S(2)}) copy-start(bf16[256,2048]{1,0:T(8,128)(2,1)} %param.15) | copy-start | bytes 3145732
  160.6 4.9 %copy-start.4 = (bf16[16,64,4096]{2,1,0:T(8,128)(2,1)}, bf16[16,64,4096]{2,1,0:T(8,128)(2,1)S(1)}, u32[]{:S(2)}) copy-start(bf16[16,64,4096]{2,1,0:T(8,128)(2,1)S(1)} %all_to_all.35) | copy-start | bytes 25165828
  160.6 2.6 copy-start.5
  163.1 2.4 copy-start.16
  163.1 2.6 copy-start.15
  165.7 2.8 copy-start.18
  177.6 80.2 %copy-start.7 = (bf16[128,256]{1,0:T(8,128)(2,1)S(1)}, bf16[128,256]{1,0:T(8,128)(2,1)}, u32[]{:S(2)}) copy-start(bf16[128,256]{1,0:T(8,128)(2,1)} %param.27) | copy-start | bytes 196612
  177.6 80.4 %copy-start.8 = (bf16[128,256]{1,0:T(8,128)(2,1)S(1)}, bf16[128,256]{1,0:T(8,128)(2,1)}, u32[]{:S(2)}) copy-start(bf16[128,256]{1,0:T(8,128)(2,1)} %param.25) | copy-start | bytes 196612
  177.6 80.5 %copy-start.9 = (bf16[128,256]{1,0:T(8,128)(2,1)S(1)}, bf16[128,256]{1,0:T(8,128)(2,1)}, u32[]{:S(2)}) copy-start(bf16[128,256]{1,0:T(8,128)(2,1)} %param.26) | copy-start | bytes 196612
  177.6 80.6 %copy-start.10 = (f32[31,128]{1,0:T(8,128)S(1)}, f32[31,128]{1,0:T(8,128)}, u32[]{:S(2)}) copy-start(f32[31,128]{1,0:T(8,128)} %param.24) | copy-start | bytes 47620
  177.6 118.7 %all-gather.3.cloned.1.call-start = ((), (), s32[]{:S(2)}) async-start(), calls=%async_computation.6 | async-start | bytes 4456448 | tf_op jit(solution)/shard_map/all_gather | solution.py:139
  258.2 5.9 %copy-start.17 = (f32[1024,384]{1,0:T(8,128)S(1)}, f32[1024,384]{1,0:T(8,128)}, u32[]{:S(2)}) copy-start(f32[1024,384]{1,0:T(8,128)} %copy-done.16) | copy-start | bytes 4718596
  258.3 5.9 %copy-start.19 = (f32[1024,384]{1,0:T(8,128)S(1)}, f32[1024,384]{1,0:T(8,128)}, u32[]{:S(2)}) copy-start(f32[1024,384]{1,0:T(8,128)} %copy-done.18) | copy-start | bytes 4718596
  319.0 8.7 %copy-start.3 = (bf16[256,2048]{1,0:T(8,128)(2,1)S(1)}, bf16[256,2048]{1,0:T(8,128)(2,1)}, u32[]{:S(2)}) copy-start(bf16[256,2048]{1,0:T(8,128)(2,1)} %param.16) | copy-start | bytes 3145732
  319.0 8.7 %copy-start.6 = (bf16[2048,128]{1,0:T(8,128)(2,1)S(1)}, bf16[2048,128]{1,0:T(8,128)(2,1)}, u32[]{:S(2)}) copy-start(bf16[2048,128]{1,0:T(8,128)(2,1)} %param.22) | copy-start | bytes 1572868
  319.0 8.7 %copy-start.11 = (f32[256]{0:T(256)S(1)}, f32[256]{0:T(256)}, u32[]{:S(2)}) copy-start(f32[256]{0:T(256)} %param.29) | copy-start | bytes 3076
  319.0 8.7 %copy-start.12 = (f32[256]{0:T(256)S(1)}, f32[256]{0:T(256)}, u32[]{:S(2)}) copy-start(f32[256]{0:T(256)} %param.28) | copy-start | bytes 3076
  319.0 8.7 %copy-start.14 = (f32[128]{0:T(128)S(1)}, f32[128]{0:T(128)}, u32[]{:S(2)}) copy-start(f32[128]{0:T(128)} %param.23) | copy-start | bytes 1540
  330.5 12.1 %all-to-all-start.3 = ((f32[16,1,512]{2,1,0:T(1,128)}), f32[16,1,512]{2,1,0:T(1,128)S(1)}, u32[]{:S(2)}, u32[]{:S(2)}) async-start(f32[16,1,512]{2,1,0:T(1,128)} %broadcast_in_dim.51), calls=%async_computation.4 | async-start | bytes 65536 | tf_op jit(solution)/shard_map/all_to_all | solution.py:38
  342.5 20.2 %all-to-all-start.2 = ((bf16[16,128,128]{2,1,0:T(8,128)(2,1)}), bf16[16,128,128]{2,1,0:T(8,128)(2,1)S(1)}, u32[]{:S(2)}, u32[]{:S(2)}) async-start(bf16[16,128,128]{2,1,0:T(8,128)(2,1)} %bitcast.16), calls=%async_computation.3 | async-start | bytes 1048576 | tf_op jit(solution)/shard_map/all_to_all | solution.py:32
  350.0 10.7 %collective-permute-start = (f32[128,30]{0,1:T(8,128)S(1)}, f32[128,30]{0,1:T(8,128)S(1)}, u32[]{:S(2)}, u32[]{:S(2)}) collective-permute-start(f32[128,30]{0,1:T(8,128)S(1)} %slice.271), channel_id=1, source_target_pairs={{16,0},{32,16},{48,32},{64,48},{80,64},{96,80},{112,96},{128,112},... | collective-permute-start | bytes 46088 | tf_op jit(solution)/shard_map/ppermute | solution.py:58
  354.9 8.5 %copy-start.1 = (bf16[1,2048,384]{2,1,0:T(8,128)(2,1)S(1)}, bf16[1,2048,384]{2,1,0:T(8,128)(2,1)}, u32[]{:S(2)}) copy-start(bf16[1,2048,384]{2,1,0:T(8,128)(2,1)} %param.19) | copy-start | bytes 4718596
Sparse Core Ops, SparseCore 0:
  177.7 64.3 reduce-scatter.1
  257.9 38.3 all-gather.2
where the time goes:
time: 377 us; the launch traced here: 370 us
  blocking collectives  115 us (31%)
  waiting for transfers between devices  95.9 us (25%)
  local copies, waits for them, and re-layouts  64.5 us (17%)
  matrix products  34.5 us (9%)
  other arithmetic  29.5 us (8%)
  starting transfers between devices  16.6 us (4%)
  between operations  14.6 us (4%)
    all_to_all x1, blocking collectives, in_one_piece(): lax.all_to_all(both, axis, split_axis=split_dim, concat_axis=concat_dim,...  101 us
    reduce_scatter x1, waiting for transfers between devices, on_device(): lax.psum_scatter(blocks.astype(jnp.bfloat16), 'tp', scatter_dimension=2,...  64.5 us
    dot_general x8, matrix products, contract(): lax.dot_general(left, right, (((left_dim,), (right_dim,)), ((), ())), pre...  29.9 us
    all_gather x1, waiting for transfers between devices, on_device(): lax.all_gather(returned.astype(jnp.bfloat16), 'tp', axis=2, tiled=True)  26.8 us
    reshape x2, local copies, waits for them, and re-layouts, on_device(): whole.reshape(expert_count * capacity, D)[target].reshape(tokens_here, 2, D)  13.9 us
    all_to_all x1, blocking collectives, on_device(): lax.all_to_all(share.astype(jnp.bfloat16), 'sp', split_axis=1, concat_axi...  13.6 us
    mul x3, local copies, waits for them, and re-layouts, on_device(): route_weight[:, :, None] * cotangent.astype(jnp.float32)[:, None, :]  11.6 us
    gather x1, local copies, waits for them, and re-layouts, on_device(): scaled[pair_index]  10.8 us
  transfers between devices with their start and end apart: 5, of which 3 were waited for; matrix products, arithmetic and copies ran while one was open for 6% of the time, Pallas kernels for 0%

commit v1 on v0

--- a/solution.py
+++ b/solution.py
@@ -136,9 +136,12 @@
     returned = lax.all_to_all(
         share.astype(jnp.bfloat16), "sp", split_axis=1, concat_axis=0, tiled=True
     ).astype(share.dtype)
-    whole = lax.all_gather(returned.astype(jnp.bfloat16), "tp", axis=2, tiled=True).astype(
-        returned.dtype
-    )
+    whole = jnp.concatenate(
+        lax.all_to_all(
+            jnp.stack([returned.astype(jnp.bfloat16)] * lax.axis_size("tp")), "tp", 0, 0
+        ),
+        axis=2,
+    ).astype(returned.dtype)
     routed = whole.reshape(expert_count * capacity, D)[target].reshape(tokens_here, 2, D)
     summed = jnp.sum(routed, axis=1)
     mixed_cot = (cotangent.astype(jnp.float32) + summed).astype(jnp.bfloat16)

time: 377 us -> 459 us (1.22)
  waiting for transfers between devices: 95.9 us -> 152 us
  local copies, waits for them, and re-layouts: 64.5 us -> 80.3 us
  other arithmetic: 29.5 us -> 36.6 us
    all_to_all x0 -> x1, waiting for transfers between devices: none -> 82.7 us  [on_device(): lax.all_to_all(jnp.stack([returned.astype(jnp.bfloat16)] * lax.axis_size(...]
    all_gather x1 -> x0, waiting for transfers between devices: 26.8 us -> none  [on_device(): lax.all_gather(returned.astype(jnp.bfloat16), 'tp', axis=2, tiled=True)]
    convert_element_type x0 -> x2, local copies, waits for them, and re-layouts: none -> 20.3 us  [on_device(): whole = jnp.concatenate(lax.all_to_all(jnp.stack([returned.astype(jnp.bfl...]
    reshape x2 -> x1, local copies, waits for them, and re-layouts: 13.9 us -> 6.03 us  [on_device(): whole.reshape(expert_count * capacity, D)[target].reshape(tokens_here, 2, D)]
    convert_element_type x0 -> x1, other arithmetic: none -> 7.07 us  [on_device(): whole = jnp.concatenate(lax.all_to_all(jnp.stack([returned.astype(jnp.bfl...]
    all_to_all x0 -> x1, starting transfers between devices: none -> 4.69 us  [on_device(): lax.all_to_all(jnp.stack([returned.astype(jnp.bfloat16)] * lax.axis_size(...]
  transfers between devices with their start and end apart: 5 -> 5, of which waited for: 3 -> 3; matrix products, arithmetic and copies ran while one was open for 6% -> 5% of each run, Pallas kernels for 0% -> 0%
where the time goes in v1:
time: 459 us; the launch traced here: 453 us
  waiting for transfers between devices  152 us (33%)
  blocking collectives  115 us (25%)
  local copies, waits for them, and re-layouts  80.3 us (17%)
  other arithmetic  36.6 us (8%)
  matrix products  34.4 us (7%)
  starting transfers between devices  20 us (4%)
  between operations  14.6 us (3%)
    all_to_all x1, blocking collectives, in_one_piece(): lax.all_to_all(both, axis, split_axis=split_dim, concat_axis=concat_dim,...  101 us
    all_to_all x1, waiting for transfers between devices, on_device(): lax.all_to_all(jnp.stack([returned.astype(jnp.bfloat16)] * lax.axis_size(...  82.7 us
    reduce_scatter x1, waiting for transfers between devices, on_device(): lax.psum_scatter(blocks.astype(jnp.bfloat16), 'tp', scatter_dimension=2,...  64.6 us
    dot_general x8, matrix products, contract(): lax.dot_general(left, right, (((left_dim,), (right_dim,)), ((), ())), pre...  29.7 us
    convert_element_type x2, local copies, waits for them, and re-layouts, on_device(): whole = jnp.concatenate(lax.all_to_all(jnp.stack([returned.astype(jnp.bfl...  20.3 us
    all_to_all x1, blocking collectives, on_device(): lax.all_to_all(share.astype(jnp.bfloat16), 'sp', split_axis=1, concat_axi...  13.6 us
    mul x3, local copies, waits for them, and re-layouts, on_device(): route_weight[:, :, None] * cotangent.astype(jnp.float32)[:, None, :]  11.6 us
    gather x1, local copies, waits for them, and re-layouts, on_device(): scaled[pair_index]  10.8 us
  transfers between devices with their start and end apart: 5, of which 3 were waited for; matrix products, arithmetic and copies ran while one was open for 5% of the time, Pallas kernels for 0%

profile of v1, /device:TPU:24, one launch (start us, length us, event | category | flops | bytes accessed | tf_op | source)
XLA Modules:
  0.0 452.5 jit_solution(16937218943977168284)
XLA Ops:
  7.2 0.0 copy-start
  7.2 0.0 reduce-scatter.2.cloned.1.call-start
  7.2 0.8 broadcast_multiply_fusion
  8.0 0.8 copy.63
  8.8 0.1 eq.25
  9.0 0.1 eq.29
  9.1 0.1 copy.62
  9.3 0.1 mul.436
  9.4 1.2 reduce-window.6
  10.6 0.2 slice_reduce_fusion
  10.9 0.1 fusion.114
  11.0 2.4 scatter_custom_fusion
  13.5 5.3 %mul.440 = f32[256,2,2048]{2,1,0:T(2,128)} broadcast(bf16[256,2048]{1,0:T(8,128)(2,1)} %param.16), dimensions={0,2} | broadcast | bytes 5242880 | tf_op jit(solution)/shard_map/mul | solution.py:117
  18.8 6.1 %mul.441 = f32[512,2048]{1,0:T(8,128)} reshape(f32[256,2,2048]{2,1,0:T(2,128)} %mul.440) | data formatting | bytes 8388608 | tf_op jit(solution)/shard_map/mul | solution.py:117
  24.9 0.1 copy.66
  25.0 0.1 mul.438
  25.2 0.1 broadcast_in_dim.46
  25.2 3.8 multiply_convert_fusion
  29.0 10.8 %gather_fusion = bf16[1024,2048]{1,0:T(8,128)(2,1)} fusion(bf16[512,2048]{1,0:T(8,128)(2,1)} %multiply_convert_fusion, s32[1024]{0:T(1024)S(1)} %get-tuple-element.73), kind=kCustom, calls=%fused_computation | custom fusion | bytes 8392704 | tf_op jit(solution)/shard_map/gather | solution.py:121
  39.8 6.0 %gather_fusion.1 = bf16[1024,2048]{1,0:T(8,128)(2,1)} fusion(bf16[256,2048]{1,0:T(8,128)(2,1)S(1)} %copy-done.2, s32[1024]{0:T(1024)S(1)} %get-tuple-element.74), kind=kCustom, calls=%fused_computation.1 | custom fusion | bytes 8392704 | tf_op jit(solution)/shard_map/gather | solution.py:124
  45.8 5.8 %broadcast_select_fusion.1 = (bf16[16,64,2048]{2,1,0:T(8,128)(2,1)}, bf16[16,64,2048]{2,1,0:T(8,128)(2,1)}) fusion(bf16[16,64,2048]{2,1,0:T(8,128)(2,1)} %bitcast.147, pred[16,64]{1,0:T(8,128)(4,1)S(1)} %broadcast_in_dim.46, bf16[16,64,2048]{2,1,0:T(8,128)(2,1)} %bitcast.148), kind=kLoop, calls=%fused_computation.11 | loop fusion | flops 4194304 | bytes 16778240 | tf_op jit(solution)/shard_map/jit(_where)/select_n | solution.py:121
  51.6 7.8 %pad_maximum_fusion = bf16[16,64,4096]{2,1,0:T(8,128)(2,1)} fusion(bf16[16,64,2048]{2,1,0:T(8,128)(2,1)} %get-tuple-element.78, bf16[16,64,2048]{2,1,0:T(8,128)(2,1)} %get-tuple-element.77), kind=kLoop, calls=%fused_computation.4 | loop fusion | flops 16777216 | bytes 16777216 | tf_op jit(solution)/shard_map/concatenate | solution.py:15
  59.4 101.1 %all_to_all.37 = bf16[16,64,4096]{2,1,0:T(8,128)(2,1)S(1)} all-to-all(bf16[16,64,4096]{2,1,0:T(8,128)(2,1)} %pad_maximum_fusion), channel_id=1, replica_groups=mesh['sp'=16,'tp'=16] {'sp'}, dimensions={0} | all-to-all | bytes 16777216 | tf_op jit(solution)/shard_map/all_to_all | solution.py:18
  160.6 2.3 fusion.3
  162.9 0.2 copy-done.5
  163.1 2.3 fusion.4
  165.5 0.2 copy-done.15
  165.7 2.8 multiply_convert_fusion.2
  168.5 2.4 fusion.8
  170.9 2.4 add_convert_fusion
  173.3 4.3 copy.67
  177.5 0.0 reduce-scatter.2.cloned.1.call-update
  177.6 64.6 %reduce-scatter.2.cloned.1.call-done = bf16[1,16,4,2048]{3,1,0,2:T(8,128)(2,1)} async-done(((bf16[1,16,64,2048]{3,1,0,2:T(8,128)(2,1)}), bf16[1,16,4,2048]{3,1,0,2:T(8,128)(2,1)}) %reduce-scatter.2.cloned.1.call-update) | async-done | bytes 262160 | tf_op jit(solution)/shard_map/reduce_scatter | solution.py:133
  242.1 1.2 copy.68
  243.3 13.6 %all_to_all.38 = bf16[1,16,4,2048]{3,2,0,1:T(4,128)(2,1)S(1)} all-to-all(bf16[1,16,4,2048]{3,2,0,1:T(4,128)(2,1)S(1)} %copy.68), channel_id=1, replica_groups=mesh['sp'=16,'tp'=16] {'sp'}, dimensions={1} | all-to-all | bytes 524288 | tf_op jit(solution)/shard_map/all_to_all | solution.py:136
  256.9 4.1 stack.14
  261.0 4.7 %all-to-all-start.2 = ((bf16[16,16,1,4,2048]{4,3,1,2,0:T(4,128)(2,1)}), bf16[16,16,1,4,2048]{4,3,1,2,0:T(4,128)(2,1)}, u32[]{:S(2)}, u32[]{:S(2)}) async-start(bf16[16,16,1,4,2048]{4,3,1,2,0:T(4,128)(2,1)} %stack.14), calls=%async_computation.3 | async-start | bytes 8388608 | tf_op jit(solution)/shard_map/all_to_all | solution.py:140
  265.7 0.1 copy.70
  265.8 0.1 copy.73
  266.0 0.1 copy.72
  266.1 0.0 copy-start.17
  266.1 0.0 copy-start.19
  266.2 5.9 %fusion.5 = bf16[1,2048,384]{2,1,0:T(8,128)(2,1)} fusion(bf16[1024,384]{1,0:T(8,128)(2,1)S(1)} %get-tuple-element.41, bf16[1,1024,4096]{2,1,0:T(8,128)(2,1)} %bitcast.153), kind=kOutput, calls=%fused_computation.19 | convolution fusion | flops 1611399168 | bytes 6553600 | tf_op jit(solution)/shard_map/dot_general | solution.py:62
  272.0 5.2 %fusion.7 = bf16[1,384,2048]{2,1,0:T(8,128)(2,1)} fusion(bf16[1,1024,4096]{2,1,0:T(8,128)(2,1)} %bitcast.154, f32[1024,384]{1,0:T(8,128)S(1)} %copy-done.19, f32[1024,384]{1,0:T(8,128)S(1)} %copy-done.17), kind=kOutput, calls=%fused_computation.21 | convolution fusion | flops 1613758464 | bytes 8912896 | tf_op jit(solution)/shard_map/dot_general | solution.py:62
  277.3 82.7 %all-to-all-done.2 = bf16[16,16,1,4,2048]{4,3,1,2,0:T(4,128)(2,1)} async-done(((bf16[16,16,1,4,2048]{4,3,1,2,0:T(4,128)(2,1)}), bf16[16,16,1,4,2048]{4,3,1,2,0:T(4,128)(2,1)}, u32[]{:S(2)}, u32[]{:S(2)}) %all-to-all-start.2) | async-done | bytes 4194336 | tf_op jit(solution)/shard_map/all_to_all | solution.py:140
  359.9 7.1 %convert_bitcast_fusion = f32[16,1,16,4,2048]{4,3,0,1,2:T(4,128)} fusion(bf16[16,16,1,4,2048]{4,3,1,2,0:T(4,128)(2,1)} %all-to-all-done.2), kind=kLoop, calls=%fused_computation.5 | loop fusion | flops 2097152 | bytes 12582912 | tf_op jit(solution)/shard_map/convert_element_type | solution.py:144
  367.0 10.3 %copy.69 = f32[16,1,16,4,2048]{4,3,2,0,1:T(4,128)} copy(f32[16,1,16,4,2048]{4,3,0,1,2:T(4,128)} %convert_bitcast_fusion) | data formatting | bytes 16777216 | tf_op jit(solution)/shard_map/convert_element_type | solution.py:144
  377.3 10.0 %reshape.166 = f32[1024,2048]{1,0:T(8,128)} reshape(f32[16,1,16,4,2048]{4,3,2,0,1:T(4,128)} %copy.69) | data formatting | bytes 16777216 | tf_op jit(solution)/shard_map/convert_element_type | solution.py:144
  387.3 8.8 %gather_fusion.2 = f32[512,2048]{1,0:T(8,128)} fusion(f32[1024,2048]{1,0:T(8,128)} %reshape.166, s32[1024]{0:T(1024)S(1)} %pad_clamp_fusion), kind=kCustom, calls=%fused_computation.2 | custom fusion | bytes 8390656 | tf_op jit(solution)/shard_map/gather | solution.py:145
  396.1 6.0 %reshape.164 = f32[256,2,2048]{2,1,0:T(2,128)} reshape(f32[512,2048]{1,0:T(8,128)} %gather_fusion.2) | data formatting | bytes 8388608 | tf_op jit(solution)/shard_map/reshape | solution.py:145
  402.2 8.6 %reduce_sum.58 = f32[256,2048]{1,0:T(8,128)} reduce(f32[256,2,2048]{2,1,0:T(2,128)} %reshape.164, f32[]{:T(128)} %constant.44.clone.1), dimensions={1}, to_apply=%region_5.6 | reduce | flops 524288 | bytes 6291460 | tf_op jit(solution)/shard_map/reduce_sum | solution.py:146
  410.9 2.1 fusion.123
  413.0 0.6 broadcast_in_dim.51
  413.7 4.6 %all-to-all-start.4 = ((f32[16,1,512]{2,1,0:T(1,128)}), f32[16,1,512]{2,1,0:T(1,128)S(1)}, u32[]{:S(2)}, u32[]{:S(2)}) async-start(f32[16,1,512]{2,1,0:T(1,128)} %broadcast_in_dim.51), calls=%async_computation.5 | async-start | bytes 65536 | tf_op jit(solution)/shard_map/all_to_all | solution.py:38
  418.3 3.1 convolution_convert_fusion.2
  421.4 4.6 %all-to-all-done.4 = f32[16,1,512]{2,1,0:T(1,128)S(1)} async-done(((f32[16,1,512]{2,1,0:T(1,128)}), f32[16,1,512]{2,1,0:T(1,128)S(1)}, u32[]{:S(2)}, u32[]{:S(2)}) %all-to-all-start.4) | async-done | bytes 32800 | tf_op jit(solution)/shard_map/all_to_all | solution.py:38
  426.0 5.8 %all-to-all-start.3 = ((bf16[16,128,128]{2,1,0:T(8,128)(2,1)}), bf16[16,128,128]{2,1,0:T(8,128)(2,1)S(1)}, u32[]{:S(2)}, u32[]{:S(2)}) async-start(bf16[16,128,128]{2,1,0:T(8,128)(2,1)} %bitcast.17), calls=%async_computation.4 | async-start | bytes 1048576 | tf_op jit(solution)/shard_map/all_to_all | solution.py:32
  431.9 0.2 subtract_multiply_fusion
  432.1 4.9 %collective-permute-start = (f32[128,30]{0,1:T(8,128)S(1)}, f32[128,30]{0,1:T(8,128)S(1)}, u32[]{:S(2)}, u32[]{:S(2)}) collective-permute-start(f32[128,30]{0,1:T(8,128)S(1)} %slice.271), channel_id=1, source_target_pairs={{16,0},{32,16},{48,32},{64,48},{80,64},{96,80},{112,96},{128,112},... | collective-permute-start | bytes 46088 | tf_op jit(solution)/shard_map/ppermute | solution.py:58
  437.0 5.8 %fusion.6 = bf16[1,2048,384]{2,1,0:T(8,128)(2,1)} fusion(bf16[1024,384]{1,0:T(8,128)(2,1)S(1)} %get-tuple-element.40, bf16[1,1024,4096]{2,1,0:T(8,128)(2,1)} %bitcast.155), kind=kOutput, calls=%fused_computation.20 | convolution fusion | flops 1611399168 | bytes 6553600 | tf_op jit(solution)/shard_map/dot_general | solution.py:62
  442.8 0.4 multiply_convert_fusion.5
  443.3 0.7 copy.74
  444.0 0.7 copy.75
  444.8 0.7 convert_reduce_fusion
  (52 shorter events, 0.3 us)
Async XLA Ops:
  7.2 153.4 %copy-start = (bf16[1,2048,384]{2,1,0:T(8,128)(2,1)S(1)}, bf16[1,2048,384]{2,1,0:T(8,128)(2,1)}, u32[]{:S(2)}) copy-start(bf16[1,2048,384]{2,1,0:T(8,128)(2,1)} %param.19) | copy-start | bytes 4718596
  7.2 234.9 %reduce-scatter.2.cloned.1.call-start = ((), (), s32[]{:S(2)}) async-start(), calls=%async_computation.6 | async-start | bytes 4456448 | tf_op jit(solution)/shard_map/reduce_scatter | solution.py:133
  18.8 6.1 %copy-start.13 = (f32[256,2]{0,1:T(2,128)S(1)}, f32[256,2]{0,1:T(2,128)}, u32[]{:S(2)}) copy-start(f32[256,2]{0,1:T(2,128)} %param.18) | copy-start | bytes 6148
  29.0 10.8 %copy-start.2 = (bf16[256,2048]{1,0:T(8,128)(2,1)S(1)}, bf16[256,2048]{1,0:T(8,128)(2,1)}, u32[]{:S(2)}) copy-start(bf16[256,2048]{1,0:T(8,128)(2,1)} %param.15) | copy-start | bytes 3145732
  160.5 4.9 %copy-start.4 = (bf16[16,64,4096]{2,1,0:T(8,128)(2,1)}, bf16[16,64,4096]{2,1,0:T(8,128)(2,1)S(1)}, u32[]{:S(2)}) copy-start(bf16[16,64,4096]{2,1,0:T(8,128)(2,1)S(1)} %all_to_all.37) | copy-start | bytes 25165828
  160.5 2.6 copy-start.5
  163.1 2.4 copy-start.16
  163.1 2.6 copy-start.15
  165.7 2.8 copy-start.18
  261.0 4.7 %copy-start.7 = (bf16[128,256]{1,0:T(8,128)(2,1)S(1)}, bf16[128,256]{1,0:T(8,128)(2,1)}, u32[]{:S(2)}) copy-start(bf16[128,256]{1,0:T(8,128)(2,1)} %param.27) | copy-start | bytes 196612
  261.0 4.8 %copy-start.8 = (bf16[128,256]{1,0:T(8,128)(2,1)S(1)}, bf16[128,256]{1,0:T(8,128)(2,1)}, u32[]{:S(2)}) copy-start(bf16[128,256]{1,0:T(8,128)(2,1)} %param.25) | copy-start | bytes 196612
  261.0 5.0 %copy-start.9 = (bf16[128,256]{1,0:T(8,128)(2,1)S(1)}, bf16[128,256]{1,0:T(8,128)(2,1)}, u32[]{:S(2)}) copy-start(bf16[128,256]{1,0:T(8,128)(2,1)} %param.26) | copy-start | bytes 196612
  261.0 5.1 %copy-start.10 = (f32[31,128]{1,0:T(8,128)S(1)}, f32[31,128]{1,0:T(8,128)}, u32[]{:S(2)}) copy-start(f32[31,128]{1,0:T(8,128)} %param.24) | copy-start | bytes 47620
  261.0 98.9 %all-to-all-start.2 = ((bf16[16,16,1,4,2048]{4,3,1,2,0:T(4,128)(2,1)}), bf16[16,16,1,4,2048]{4,3,1,2,0:T(4,128)(2,1)}, u32[]{:S(2)}, u32[]{:S(2)}) async-start(bf16[16,16,1,4,2048]{4,3,1,2,0:T(4,128)(2,1)} %stack.14), calls=%async_computation.3 | async-start | bytes 8388608 | tf_op jit(solution)/shard_map/all_to_all | solution.py:140
  266.1 5.9 %copy-start.17 = (f32[1024,384]{1,0:T(8,128)S(1)}, f32[1024,384]{1,0:T(8,128)}, u32[]{:S(2)}) copy-start(f32[1024,384]{1,0:T(8,128)} %copy-done.16) | copy-start | bytes 4718596
  266.1 5.9 %copy-start.19 = (f32[1024,384]{1,0:T(8,128)S(1)}, f32[1024,384]{1,0:T(8,128)}, u32[]{:S(2)}) copy-start(f32[1024,384]{1,0:T(8,128)} %copy-done.18) | copy-start | bytes 4718596
  402.2 8.7 %copy-start.3 = (bf16[256,2048]{1,0:T(8,128)(2,1)S(1)}, bf16[256,2048]{1,0:T(8,128)(2,1)}, u32[]{:S(2)}) copy-start(bf16[256,2048]{1,0:T(8,128)(2,1)} %param.16) | copy-start | bytes 3145732
  402.2 8.7 %copy-start.6 = (bf16[2048,128]{1,0:T(8,128)(2,1)S(1)}, bf16[2048,128]{1,0:T(8,128)(2,1)}, u32[]{:S(2)}) copy-start(bf16[2048,128]{1,0:T(8,128)(2,1)} %param.22) | copy-start | bytes 1572868
  402.2 8.7 %copy-start.11 = (f32[256]{0:T(256)S(1)}, f32[256]{0:T(256)}, u32[]{:S(2)}) copy-start(f32[256]{0:T(256)} %param.29) | copy-start | bytes 3076
  402.2 8.7 %copy-start.12 = (f32[256]{0:T(256)S(1)}, f32[256]{0:T(256)}, u32[]{:S(2)}) copy-start(f32[256]{0:T(256)} %param.28) | copy-start | bytes 3076
  402.2 8.7 %copy-start.14 = (f32[128]{0:T(128)S(1)}, f32[128]{0:T(128)}, u32[]{:S(2)}) copy-start(f32[128]{0:T(128)} %param.23) | copy-start | bytes 1540
  413.7 12.3 %all-to-all-start.4 = ((f32[16,1,512]{2,1,0:T(1,128)}), f32[16,1,512]{2,1,0:T(1,128)S(1)}, u32[]{:S(2)}, u32[]{:S(2)}) async-start(f32[16,1,512]{2,1,0:T(1,128)} %broadcast_in_dim.51), calls=%async_computation.5 | async-start | bytes 65536 | tf_op jit(solution)/shard_map/all_to_all | solution.py:38
  426.0 18.8 %all-to-all-start.3 = ((bf16[16,128,128]{2,1,0:T(8,128)(2,1)}), bf16[16,128,128]{2,1,0:T(8,128)(2,1)S(1)}, u32[]{:S(2)}, u32[]{:S(2)}) async-start(bf16[16,128,128]{2,1,0:T(8,128)(2,1)} %bitcast.17), calls=%async_computation.4 | async-start | bytes 1048576 | tf_op jit(solution)/shard_map/all_to_all | solution.py:32
  432.1 10.7 %collective-permute-start = (f32[128,30]{0,1:T(8,128)S(1)}, f32[128,30]{0,1:T(8,128)S(1)}, u32[]{:S(2)}, u32[]{:S(2)}) collective-permute-start(f32[128,30]{0,1:T(8,128)S(1)} %slice.271), channel_id=1, source_target_pairs={{16,0},{32,16},{48,32},{64,48},{80,64},{96,80},{112,96},{128,112},... | collective-permute-start | bytes 46088 | tf_op jit(solution)/shard_map/ppermute | solution.py:58
  437.0 8.5 %copy-start.1 = (bf16[1,2048,384]{2,1,0:T(8,128)(2,1)S(1)}, bf16[1,2048,384]{2,1,0:T(8,128)(2,1)}, u32[]{:S(2)}) copy-start(bf16[1,2048,384]{2,1,0:T(8,128)(2,1)} %param.19) | copy-start | bytes 4718596
Sparse Core Ops, SparseCore 0:
  177.7 64.3 reduce-scatter.1
